TPU v7x, 32 devices: a whole 2x2x4 slice. The times are simulated.
32 devices in a mesh: rep: 4 (over z), fs: 4 (over y, x), tp: 2 (over core).
Axes of the slice: x: 2, y: 2, z: 4, core: 2. Of those that a mesh axis runs over, the one named last changes fastest.
Arguments:
- tokens: bfloat16 [2048, 1024], P(('rep', 'fs', 'tp')), may hold values from -6 to 6
- cotangent: bfloat16 [2048, 1024], P(('rep', 'fs', 'tp')), may hold values from -6 to 6
- gate_weight: bfloat16 [1024, 2816], P('fs', 'tp'), may hold values from -0.1875 to 0.1875
- up_weight: bfloat16 [1024, 2816], P('fs', 'tp'), may hold values from -0.1875 to 0.1875
- down_weight: bfloat16 [2816, 1024], P('tp', 'fs'), may hold values from -0.109375 to 0.109375
Outputs:
- input_grad: bfloat16 [2048, 1024], P(('rep', 'fs', 'tp'))
- gate_grad: float32 [1024, 2816], P('fs', 'tp')
- up_grad: float32 [1024, 2816], P('fs', 'tp')
- down_grad: float32 [2816, 1024], P('tp', 'fs')
- gate_power: float32 [1024], P('fs')
- up_power: float32 [1024], P('fs')
- down_power: float32 [2816], P('tp')
All inputs are finite; a program needn't handle non-finite values.
Results may differ from a plain program's by a relative error of at most 0.0017.
Values may be sent and summed in bfloat16 or wider, within the bound.
A program may use at most 64 MiB of HBM per device.

v0:
```python
import math
import jax
import jax.numpy as jnp
from jax import lax
from jax.sharding import PartitionSpec as P

D = 1024
FF = 2816
EPSILON = 1e-06


def contract_rows(left, right):
    return lax.dot_general(
        left, right, (((0,), (0,)), ((), ())), preferred_element_type=jnp.float32
    )


def contract_cols(left, right):
    return lax.dot_general(
        left, right, (((1,), (1,)), ((), ())), preferred_element_type=jnp.float32
    )


def on_device(tokens, cotangent, gate_weight, up_weight, down_weight):
    tp_count = lax.axis_size("tp")
    fs_count = lax.axis_size("fs")
    rep_count = lax.axis_size("rep")
    width = tokens.shape[1]
    factor = 1.0 / math.sqrt(tokens.shape[0] * tp_count * fs_count * rep_count)
    xfloat = tokens.astype(jnp.float32)
    recip_norm = lax.rsqrt(jnp.mean(xfloat * xfloat, axis=1, keepdims=True) + EPSILON)
    normed_exact = xfloat * recip_norm
    normed = normed_exact.astype(jnp.bfloat16)
    group_normed, group_cotangent = (
        lax.all_gather(normed, "tp", axis=0, tiled=True),
        lax.all_gather(cotangent, "tp", axis=0, tiled=True),
    )
    gate_full, up_full, down_full = (
        lax.all_gather(gate_weight, "fs", axis=0, tiled=True),
        lax.all_gather(up_weight, "fs", axis=0, tiled=True),
        lax.all_gather(down_weight.T, "fs", axis=0, tiled=True),
    )
    gate_pre = jnp.dot(group_normed, gate_full, preferred_element_type=jnp.float32)
    up_pre = jnp.dot(group_normed, up_full, preferred_element_type=jnp.float32)
    sigmoid_gate = jax.nn.sigmoid(gate_pre)
    activated = gate_pre * sigmoid_gate
    hidden = (activated * up_pre).astype(jnp.bfloat16)
    grad_hidden = 0.5 * jnp.dot(group_cotangent, down_full, preferred_element_type=jnp.float32)
    grad_up_pre = (grad_hidden * activated).astype(jnp.bfloat16)
    grad_gate_pre = (
        grad_hidden * up_pre * sigmoid_gate * (1.0 + gate_pre * (1.0 - sigmoid_gate))
    ).astype(jnp.bfloat16)
    normed_part = contract_cols(grad_gate_pre, gate_full) + contract_cols(grad_up_pre, up_full)
    grad_normed = lax.psum_scatter(normed_part, "tp", scatter_dimension=0, tiled=True)
    inner = jnp.mean(grad_normed * normed_exact, axis=1, keepdims=True)
    input_grad = (recip_norm * (grad_normed - normed_exact * inner)).astype(jnp.bfloat16)
    hidden_local = gate_weight.shape[1]

    def rows_term():
        normed_cols = lax.slice_in_dim(
            group_normed, 0, width // fs_count * lax.axis_size("fs"), axis=1
        )
        cotangent_cols = lax.slice_in_dim(
            group_cotangent, 0, width // fs_count * lax.axis_size("fs"), axis=1
        )
        return factor * jnp.concatenate(
            [
                contract_rows(normed_cols, grad_gate_pre),
                contract_rows(normed_cols, grad_up_pre),
                0.5 * contract_rows(cotangent_cols, hidden),
            ],
            axis=1,
        )

    reduced = lax.psum_scatter(rows_term(), "fs", scatter_dimension=0, tiled=True)
    reduced = lax.psum(reduced, "rep")
    gate_grad = reduced[:, :hidden_local]
    up_grad = reduced[:, hidden_local : 2 * hidden_local]
    down_grad = reduced[:, 2 * hidden_local :].T
    gate_sums, up_sums = lax.psum(
        (jnp.sum(gate_grad * gate_grad, axis=1), jnp.sum(up_grad * up_grad, axis=1)), "tp"
    )
    down_sums = lax.psum(jnp.sum(down_grad * down_grad, axis=1), "fs")
    return (input_grad, gate_grad, up_grad, down_grad, gate_sums / FF, up_sums / FF, down_sums / D)


def solution(mesh):
    placed = (
        P(("rep", "fs", "tp"), None),
        P(("rep", "fs", "tp"), None),
        P("fs", "tp"),
        P("fs", "tp"),
        P("tp", "fs"),
    )
    return jax.shard_map(
        on_device,
        mesh=mesh,
        in_specs=placed,
        out_specs=(
            P(("rep", "fs", "tp"), None),
            P("fs", "tp"),
            P("fs", "tp"),
            P("tp", "fs"),
            P("fs"),
            P("fs"),
            P("tp"),
        ),
        check_vma=False,
    )
```

profile of v0, /device:TPU:0, one launch (start us, length us, event | category | flops | bytes accessed | tf_op | source)
XLA Modules:
  0.0 513.0 jit_solution(5771994517067918810)
XLA Ops:
  7.2 0.0 all-gather.8.cloned.1.call-start
  7.2 0.7 all-gather.8.cloned.1.call-update
  7.9 0.0 all-gather.6.cloned.1.call-start
  8.0 0.7 all-gather.6.cloned.1.call-update
  8.7 0.0 all-gather.4.cloned.1.call-start
  8.7 0.7 all-gather.4.cloned.1.call-update
  9.4 0.0 reduce-scatter.5.cloned.1.call-start
  9.4 1.0 fusion.8
  10.5 1.0 fusion.3
  11.5 2.1 all_gather.17
  13.6 2.0 all_gather.15
  15.6 38.7 %all-gather.8.cloned.1.call-done = bf16[1024,1408]{1,0:T(8,128)(2,1)} async-done(((bf16[256,1408]{1,0:T(8,128)(2,1)}), bf16[1024,1408]{1,0:T(8,128)(2,1)}) %all-gather.8.cloned.1.call-update) | async-done | bytes 2883600 | tf_op jit(solution)/shard_map/all_gather | solution.py:39
  54.3 2.4 fusion.12
  56.7 41.1 %all-gather.6.cloned.1.call-done = bf16[1024,1408]{1,0:T(8,128)(2,1)} async-done(((bf16[256,1408]{1,0:T(8,128)(2,1)}), bf16[1024,1408]{1,0:T(8,128)(2,1)}) %all-gather.6.cloned.1.call-update) | async-done | bytes 2883600 | tf_op jit(solution)/shard_map/all_gather | solution.py:40
  97.8 2.4 fusion.11
  100.2 3.5 multiply_bitcast_fusion
  103.7 37.5 %all-gather.4.cloned.1.call-done = bf16[1024,1408]{0,1:T(8,128)(2,1)} async-done(((bf16[256,1408]{0,1:T(8,128)(2,1)}), bf16[1024,1408]{0,1:T(8,128)(2,1)}) %all-gather.4.cloned.1.call-update) | async-done | bytes 2883600 | tf_op jit(solution)/shard_map/all_gather | solution.py:41
  141.2 2.9 multiply_convert_fusion.1
  144.1 0.0 copy-start.3
  144.2 0.9 fusion.15
  145.1 0.0 slice-start
  145.1 0.0 slice-start.1
  145.1 0.9 fusion.14
  146.1 1.2 slice-done
  147.3 0.5 slice-done.1
  147.8 6.3 %maximum_multiply_fusion = f32[1024,4224]{1,0:T(8,128)} fusion(f32[1024,1408]{1,0:T(8,128)S(1)} %bitcast.23, f32[1024,1408]{1,0:T(8,128)S(1)} %fusion.15, f32[1024,1408]{1,0:T(8,128)S(1)} %fusion.14), kind=kLoop, calls=%fused_computation | loop fusion | flops 12976128 | bytes 34603008 | tf_op jit(solution)/shard_map/mul | solution.py:66
  154.1 0.0 reduce-scatter.5.cloned.1.call-update
  154.1 0.0 reduce-scatter.3.cloned.1.call-start
  154.2 1.7 copy-done
  155.9 1.0 fusion.13
  157.0 0.8 copy-done.1
  157.7 0.0 copy-done.4
  157.7 1.8 convolution_add_fusion
  159.6 0.0 reduce-scatter.3.cloned.1.call-update
  159.6 0.0 all-reduce.3.cloned.1.call-start
  159.7 152.6 %reduce-scatter.5.cloned.1.call-done = f32[256,4224]{1,0:T(8,128)} async-done(((f32[1024,4224]{1,0:T(8,128)}), f32[256,4224]{1,0:T(8,128)}) %reduce-scatter.5.cloned.1.call-update) | async-done | bytes 4325392 | tf_op jit(solution)/shard_map/reduce_scatter | solution.py:75
  312.3 0.0 all-reduce.3.cloned.1.call-update
  312.3 10.6 %reduce-scatter.3.cloned.1.call-done = f32[64,1024]{1,0:T(8,128)} async-done(((f32[128,1024]{1,0:T(8,128)}), f32[64,1024]{1,0:T(8,128)}) %reduce-scatter.3.cloned.1.call-update) | async-done | bytes 262160 | tf_op jit(solution)/shard_map/reduce_scatter | solution.py:54
  322.9 1.2 fusion.4
  324.0 1.7 fusion.7
  325.8 159.7 %all-reduce.3.cloned.1.call-done = f32[256,4224]{1,0:T(8,128)} async-done(((f32[256,4224]{1,0:T(8,128)}), f32[256,4224]{1,0:T(8,128)}) %all-reduce.3.cloned.1.call-update) | async-done | bytes 4325392 | tf_op jit(solution)/shard_map/psum | solution.py:76
  485.5 1.5 multiply_reduce_fusion
  487.0 10.1 %psum.31 = f32[1408]{0:T(1024)S(1)} all-reduce(f32[1408]{0:T(1024)S(1)} %multiply_reduce_fusion), channel_id=1, replica_groups=mesh['rep'=4,'fs'=4,'tp'=2] {'fs'}, use_global_device_ids=true, to_apply=%region_10.0 | all-reduce | flops 1408 | bytes 11264 | tf_op jit(solution)/shard_map/psum | solution.py:83
  497.0 0.6 broadcast_multiply_fusion
  497.6 3.9 multiply_reduce_fusion.1
  501.6 1.5 copy.13
  503.1 2.4 all-reduce
  505.5 0.6 broadcast_multiply_fusion.1
  (11 shorter events, 0.0 us)
Async XLA Ops:
  7.2 6.5 %copy-start.5 = (bf16[64,1024]{1,0:T(8,128)(2,1)S(1)}, bf16[64,1024]{1,0:T(8,128)(2,1)}, u32[]{:S(2)}) copy-start(bf16[64,1024]{1,0:T(8,128)(2,1)} %param.6) | copy-start | bytes 393220
  7.2 47.1 %all-gather.8.cloned.1.call-start = ((), (), s32[]{:S(2)}) async-start(), calls=%async_computation.4 | async-start | bytes 3604480 | tf_op jit(solution)/shard_map/all_gather | solution.py:39
  7.9 89.9 %all-gather.6.cloned.1.call-start = ((), (), s32[]{:S(2)}) async-start(), calls=%async_computation.3 | async-start | bytes 3604480 | tf_op jit(solution)/shard_map/all_gather | solution.py:40
  8.7 132.5 %all-gather.4.cloned.1.call-start = ((), (), s32[]{:S(2)}) async-start(), calls=%async_computation.2 | async-start | bytes 3604480 | tf_op jit(solution)/shard_map/all_gather | solution.py:41
  9.4 302.9 %reduce-scatter.5.cloned.1.call-start = ((), (), s32[]{:S(2)}) async-start(), calls=%async_computation.6 | async-start | bytes 21626880 | tf_op jit(solution)/shard_map/reduce_scatter | solution.py:75
  144.1 1.0 copy-start.3
  145.1 2.2 slice-start
  145.1 2.7 slice-start.1
  154.1 1.8 copy-start
  154.1 168.8 %reduce-scatter.3.cloned.1.call-start = ((), (), s32[]{:S(2)}) async-start(), calls=%async_computation.5 | async-start | bytes 786432 | tf_op jit(solution)/shard_map/reduce_scatter | solution.py:54
  155.9 1.8 copy-start.1
  155.9 1.8 copy-start.4
  159.6 163.3 %copy-start.2 = (bf16[64,1024]{1,0:T(8,128)(2,1)S(1)}, bf16[64,1024]{1,0:T(8,128)(2,1)}, u32[]{:S(2)}) copy-start(bf16[64,1024]{1,0:T(8,128)(2,1)} %param.5) | copy-start | bytes 393220
  159.6 325.9 %all-reduce.3.cloned.1.call-start = ((), (), s32[]{:S(2)}) async-start(), calls=%async_computation.7 | async-start | bytes 8650752 | tf_op jit(solution)/shard_map/psum | solution.py:76
Sparse Core Ops, SparseCore 0:
  9.8 44.3 all-gather.7
  56.1 41.6 all-gather.5
  99.6 41.5 all-gather.3
  154.2 157.9 reduce-scatter.4
  314.9 7.9 reduce-scatter.2
  325.1 160.3 all-reduce.2
where the time goes:
time: 513 us
  waiting for transfers between devices  442 us (86%)
  other arithmetic  17.8 us (3%)
  blocking collectives  16.6 us (3%)
  matrix products  16 us (3%)
  between operations  14.2 us (3%)
  local copies, waits for them, and re-layouts  5.81 us (1%)
    psum x1, waiting for transfers between devices, on_device(): reduced = lax.psum(reduced, 'rep')  160 us
    reduce_scatter x1, waiting for transfers between devices, on_device(): lax.psum_scatter(rows_term(), 'fs', scatter_dimension=0, tiled=True)  153 us
    all_gather x1, waiting for transfers between devices, on_device(): lax.all_gather(up_weight, 'fs', axis=0, tiled=True)  41.1 us
    all_gather x1, waiting for transfers between devices, on_device(): lax.all_gather(gate_weight, 'fs', axis=0, tiled=True)  38.7 us
    all_gather x1, waiting for transfers between devices, on_device(): lax.all_gather(down_weight.T, 'fs', axis=0, tiled=True)  37.5 us
    reduce_scatter x1, waiting for transfers between devices, on_device(): lax.psum_scatter(normed_part, 'tp', scatter_dimension=0, tiled=True)  10.6 us
  transfers between devices with their start and end apart: 6, of which 6 were waited for; matrix products, arithmetic and copies ran while one was open for 3% of the time, Pallas kernels for 0%

commit v1 on v0

--- a/solution.py
+++ b/solution.py
@@ -7,6 +7,12 @@
 D = 1024
 FF = 2816
 EPSILON = 1e-06
+
+
+def gather_and_add(array, axis):
+    terms = lax.all_gather(array, axis, axis=0, tiled=False)
+    total = terms.sum(axis=0)
+    return total
 
 
 def contract_rows(left, right):
@@ -73,7 +79,7 @@
         )
 
     reduced = lax.psum_scatter(rows_term(), "fs", scatter_dimension=0, tiled=True)
-    reduced = lax.psum(reduced, "rep")
+    reduced = gather_and_add(reduced, "rep")
     gate_grad = reduced[:, :hidden_local]
     up_grad = reduced[:, hidden_local : 2 * hidden_local]
     down_grad = reduced[:, 2 * hidden_local :].T

time: 513 us -> 660 us (1.29)
  waiting for transfers between devices: 442 us -> 579 us
  other arithmetic: 17.8 us -> 27.1 us
    all_gather x0 -> x1, waiting for transfers between devices: none -> 297 us  [gather_and_add(): terms = lax.all_gather(array, axis, axis=0, tiled=False)]
    psum x1 -> x0, waiting for transfers between devices: 160 us -> none  [on_device(): reduced = lax.psum(reduced, 'rep')]
    reduce_sum x0 -> x1, other arithmetic: none -> 9.34 us  [gather_and_add(): total = terms.sum(axis=0)]
  transfers between devices with their start and end apart: 6 -> 6, of which waited for: 6 -> 6; matrix products, arithmetic and copies ran while one was open for 3% -> 2% of each run, Pallas kernels for 0% -> 0%
where the time goes in v1:
time: 660 us; the launch traced here: 659 us
  waiting for transfers between devices  579 us (88%)
  other arithmetic  27.1 us (4%)
  blocking collectives  16.6 us (3%)
  matrix products  15.9 us (2%)
  between operations  14.2 us (2%)
    all_gather x1, waiting for transfers between devices, gather_and_add(): terms = lax.all_gather(array, axis, axis=0, tiled=False)  297 us
    reduce_scatter x1, waiting for transfers between devices, on_device(): lax.psum_scatter(rows_term(), 'fs', scatter_dimension=0, tiled=True)  153 us
    all_gather x1, waiting for transfers between devices, on_device(): lax.all_gather(up_weight, 'fs', axis=0, tiled=True)  41.1 us
    all_gather x1, waiting for transfers between devices, on_device(): lax.all_gather(gate_weight, 'fs', axis=0, tiled=True)  38.7 us
    all_gather x1, waiting for transfers between devices, on_device(): lax.all_gather(down_weight.T, 'fs', axis=0, tiled=True)  37.5 us
  transfers between devices with their start and end apart: 6, of which 6 were waited for; matrix products, arithmetic and copies ran while one was open for 2% of the time, Pallas kernels for 0%

profile of v1, /device:TPU:0, one launch (start us, length us, event | category | flops | bytes accessed | tf_op | source)
XLA Modules:
  0.0 659.1 jit_solution(585346418188631449)
XLA Ops:
  7.2 0.0 all-gather.10.cloned.1.call-start
  7.2 0.7 all-gather.10.cloned.1.call-update
  7.9 0.0 all-gather.8.cloned.1.call-start
  8.0 0.7 all-gather.8.cloned.1.call-update
  8.7 0.0 all-gather.6.cloned.1.call-start
  8.7 0.7 all-gather.6.cloned.1.call-update
  9.4 0.0 reduce-scatter.5.cloned.1.call-start
  9.4 1.0 fusion.8
  10.5 1.0 fusion.3
  11.5 2.1 all_gather.23
  13.6 2.0 all_gather.21
  15.6 38.7 %all-gather.10.cloned.1.call-done = bf16[1024,1408]{1,0:T(8,128)(2,1)} async-done(((bf16[256,1408]{1,0:T(8,128)(2,1)}), bf16[1024,1408]{1,0:T(8,128)(2,1)}) %all-gather.10.cloned.1.call-update) | async-done | bytes 2883600 | tf_op jit(solution)/shard_map/all_gather | solution.py:45
  54.3 2.4 fusion.12
  56.7 41.1 %all-gather.8.cloned.1.call-done = bf16[1024,1408]{1,0:T(8,128)(2,1)} async-done(((bf16[256,1408]{1,0:T(8,128)(2,1)}), bf16[1024,1408]{1,0:T(8,128)(2,1)}) %all-gather.8.cloned.1.call-update) | async-done | bytes 2883600 | tf_op jit(solution)/shard_map/all_gather | solution.py:46
  97.8 2.4 fusion.11
  100.2 3.5 multiply_bitcast_fusion
  103.7 37.5 %all-gather.6.cloned.1.call-done = bf16[1024,1408]{0,1:T(8,128)(2,1)} async-done(((bf16[256,1408]{0,1:T(8,128)(2,1)}), bf16[1024,1408]{0,1:T(8,128)(2,1)}) %all-gather.6.cloned.1.call-update) | async-done | bytes 2883600 | tf_op jit(solution)/shard_map/all_gather | solution.py:47
  141.2 2.9 multiply_convert_fusion.1
  144.1 0.0 copy-start.3
  144.2 0.9 fusion.15
  145.1 0.0 slice-start.1
  145.1 0.9 fusion.14
  146.1 1.2 slice-done
  147.3 0.5 slice-done.1
  147.8 6.3 maximum_multiply_fusion
  154.1 0.0 reduce-scatter.5.cloned.1.call-update
  154.1 0.0 reduce-scatter.3.cloned.1.call-start
  154.1 1.7 copy-done
  155.9 1.0 fusion.13
  156.9 0.8 copy-done.1
  157.7 0.0 copy-done.4
  157.7 1.9 convolution_add_fusion
  159.6 0.0 reduce-scatter.3.cloned.1.call-update
  159.6 0.0 all-gather.12.cloned.1.call-start
  159.7 152.6 %reduce-scatter.5.cloned.1.call-done = f32[256,4224]{1,0:T(8,128)} async-done(((f32[1024,4224]{1,0:T(8,128)}), f32[256,4224]{1,0:T(8,128)}) %reduce-scatter.5.cloned.1.call-update) | async-done | bytes 4325392 | tf_op jit(solution)/shard_map/reduce_scatter | solution.py:81
  312.2 0.0 all-gather.12.cloned.1.call-update
  312.3 10.6 %reduce-scatter.3.cloned.1.call-done = f32[64,1024]{1,0:T(8,128)} async-done(((f32[128,1024]{1,0:T(8,128)}), f32[64,1024]{1,0:T(8,128)}) %reduce-scatter.3.cloned.1.call-update) | async-done | bytes 262160 | tf_op jit(solution)/shard_map/reduce_scatter | solution.py:60
  322.9 1.2 fusion.4
  324.0 1.7 fusion.7
  325.8 296.6 %all-gather.12.cloned.1.call-done = f32[1024,4224]{1,0:T(8,128)} async-done(((f32[256,4224]{1,0:T(8,128)}), f32[1024,4224]{1,0:T(8,128)}) %all-gather.12.cloned.1.call-update) | async-done | bytes 17301520 | tf_op jit(solution)/shard_map/all_gather | solution.py:13
  622.3 9.3 %reduce_sum.56 = f32[256,4224]{1,0:T(8,128)} reduce(f32[4,256,4224]{2,1,0:T(8,128)} %bitcast.25, f32[]{:T(128)} %constant.7.clone.1), dimensions={0}, to_apply=%region_4.0 | reduce | flops 3244032 | bytes 21626884 | tf_op jit(solution)/shard_map/reduce_sum | solution.py:14
  631.7 1.5 multiply_reduce_fusion
  633.2 3.9 multiply_reduce_fusion.1
  637.1 10.0 %psum.23 = f32[1408]{0:T(1024)S(1)} all-reduce(f32[1408]{0:T(1024)S(1)} %multiply_reduce_fusion), channel_id=1, replica_groups=mesh['rep'=4,'fs'=4,'tp'=2] {'fs'}, use_global_device_ids=true, to_apply=%region_10.0 | all-reduce | flops 1408 | bytes 11264 | tf_op jit(solution)/shard_map/psum | solution.py:89
  647.1 0.6 broadcast_multiply_fusion
  647.7 1.5 copy.16
  649.3 2.4 all-reduce
  651.7 0.6 broadcast_multiply_fusion.1
  (12 shorter events, 0.0 us)
Async XLA Ops:
  7.2 6.5 copy-start.5
  7.2 47.1 %all-gather.10.cloned.1.call-start = ((), (), s32[]{:S(2)}) async-start(), calls=%async_computation.4 | async-start | bytes 3604480 | tf_op jit(solution)/shard_map/all_gather | solution.py:45
  7.9 89.9 %all-gather.8.cloned.1.call-start = ((), (), s32[]{:S(2)}) async-start(), calls=%async_computation.3 | async-start | bytes 3604480 | tf_op jit(solution)/shard_map/all_gather | solution.py:46
  8.7 132.5 %all-gather.6.cloned.1.call-start = ((), (), s32[]{:S(2)}) async-start(), calls=%async_computation.2 | async-start | bytes 3604480 | tf_op jit(solution)/shard_map/all_gather | solution.py:47
  9.4 302.8 %reduce-scatter.5.cloned.1.call-start = ((), (), s32[]{:S(2)}) async-start(), calls=%async_computation.6 | async-start | bytes 21626880 | tf_op jit(solution)/shard_map/reduce_scatter | solution.py:81
  144.1 1.0 copy-start.3
  145.1 2.2 slice-start
  145.1 2.7 slice-start.1
  154.1 1.8 copy-start
  154.1 168.8 %reduce-scatter.3.cloned.1.call-start = ((), (), s32[]{:S(2)}) async-start(), calls=%async_computation.5 | async-start | bytes 786432 | tf_op jit(solution)/shard_map/reduce_scatter | solution.py:60
  155.9 1.8 copy-start.1
  155.9 1.8 copy-start.4
  159.6 163.3 %copy-start.2 = (bf16[64,1024]{1,0:T(8,128)(2,1)S(1)}, bf16[64,1024]{1,0:T(8,128)(2,1)}, u32[]{:S(2)}) copy-start(bf16[64,1024]{1,0:T(8,128)(2,1)} %param.5) | copy-start | bytes 393220
  159.6 462.7 %all-gather.12.cloned.1.call-start = ((), (), s32[]{:S(2)}) async-start(), calls=%async_computation.7 | async-start | bytes 21626880 | tf_op jit(solution)/shard_map/all_gather | solution.py:13
Sparse Core Ops, SparseCore 0:
  9.8 44.3 all-gather.9
  56.1 41.6 all-gather.7
  99.6 41.5 all-gather.5
  154.2 157.9 reduce-scatter.4
  314.9 7.9 reduce-scatter.2
  324.3 297.9 all-gather.11
